TPU v7x, 32 devices: a whole 2x2x4 slice. The times are simulated.
32 devices in a mesh: sp: 4 (over z), fs: 4 (over y, x), tp: 2 (over core).
Axes of the slice: x: 2, y: 2, z: 4, core: 2. Of those that a mesh axis runs over, the one named last changes fastest.
Arguments:
- tokens: bfloat16 [4, 1024, 2048], P('fs', 'sp', 'tp'), may hold values from -6 to 6
- norm_gain: float32 [2048], replicated, may hold values from 0.1 to 1.9
- ret_query: bfloat16 [2048, 1024], P('sp', 'tp'), may hold values from -0.125 to 0.125
- ret_key: bfloat16 [2048, 1024], P('sp', 'tp'), may hold values from -0.125 to 0.125
- ret_value: bfloat16 [2048, 1024], P('sp', 'tp'), may hold values from -0.125 to 0.125
- att_query: bfloat16 [2048, 1024], P('sp', 'tp'), may hold values from -0.125 to 0.125
- att_key: bfloat16 [2048, 256], P('sp', 'tp'), may hold values from -0.125 to 0.125
- att_value: bfloat16 [2048, 256], P('sp', 'tp'), may hold values from -0.125 to 0.125
- log_decay: float32 [4, 4, 1024], P('fs', 'tp', 'sp'), may hold values from -1 to 0
- start_state: float32 [4, 4, 256, 256], P('fs', 'tp'), may hold values from -12 to 12
- ret_gain: float32 [1024], P('tp'), may hold values from 0.1 to 1.9
- sink_logits: float32 [16], P('tp'), may hold values from 1 to 5
- ret_out: bfloat16 [1024, 2048], P('tp', 'fs'), may hold values from -0.1875 to 0.1875
- att_out: bfloat16 [1024, 2048], P('tp', 'fs'), may hold values from -1.5 to 1.5
Outputs:
- mixed: bfloat16 [4, 1024, 2048], P('fs', 'sp', 'tp')
All inputs are finite; a program needn't handle non-finite values.
Results may differ from a plain program's by a relative error of at most 0.015.
Values may be sent and summed in bfloat16 or wider, within the bound.
A program may use at most 128 MiB of HBM per device.

v0:
```python
import jax
import jax.numpy as jnp
from jax import lax
from jax.sharding import PartitionSpec as P

DK = 256
DV = 256
HD = 64
WINDOW = 128
BLOCK = 128
epsilon = 1e-06
exact_result = lax.Precision.HIGHEST


def carried_in(array, axis, combine, identity):
    peers, mine = (lax.axis_size(axis), lax.axis_index(axis))
    everything = jax.tree.map(
        lambda part, kind: lax.all_gather(part.astype(kind), axis),
        array,
        (jnp.bfloat16, jnp.bfloat16),
    )
    start = jax.tree.map(
        lambda part, zero: jnp.broadcast_to(jnp.asarray(zero, part.dtype), part.shape),
        array,
        identity,
    )

    def hop(k, before):
        reached = k < mine
        new = combine(
            before, jax.tree.map(lambda part, own: part[k].astype(own.dtype), everything, array)
        )
        return jax.tree.map(lambda a, b: jnp.where(reached, a, b), new, before)

    return lax.fori_loop(0, peers, hop, start)


def passed_along(block, axis, distance):
    devices = range(lax.axis_size(axis))
    route = [(i - distance, i) for i in devices if i - distance in devices]
    return lax.ppermute(block, axis, route)


def rotate(values, positions):
    half_dim = values.shape[-1] // 2
    inverse = 1.0 / 10000.0 ** (jnp.arange(half_dim, dtype=jnp.float32) / half_dim)
    angles = positions.astype(jnp.float32)[:, None] * inverse[None, :]
    cosine = jnp.cos(angles)[:, None, :]
    sine_table = jnp.sin(angles)[:, None, :]
    front_half = values[..., :half_dim]
    back_half = values[..., half_dim:]
    return jnp.concatenate(
        [
            front_half * cosine - back_half * sine_table,
            front_half * sine_table + back_half * cosine,
        ],
        axis=-1,
    )


def block_step(memory_state, inputs):
    queries, key_matrix_rows, value_matrix_rows, log_rates = inputs
    length_here = log_rates.shape[-1]
    causal = jnp.arange(length_here)[:, None] >= jnp.arange(length_here)[None, :]
    running_totals = jnp.cumsum(log_rates, axis=-1)
    relative = running_totals[:, :, None] - running_totals[:, None, :]
    weight = jnp.where(causal[None], jnp.exp(jnp.where(causal[None], relative, 0.0)), 0.0)
    score_matrix = (
        jnp.einsum("hqd,hkd->hqk", queries, key_matrix_rows, precision=exact_result) * weight
    )
    carried_state = jnp.einsum(
        "hqd,hdv->hqv",
        queries * jnp.exp(running_totals)[:, :, None],
        memory_state,
        precision=exact_result,
    )
    output_rows = (
        jnp.einsum("arf,afu->aru", score_matrix, value_matrix_rows, precision=exact_result)
        + carried_state
    )
    decay_factors = jnp.exp(running_totals[:, -1:] - running_totals)
    memory_state = memory_state * jnp.exp(running_totals[:, -1])[:, None, None] + jnp.einsum(
        "iwj,iwe->ije",
        key_matrix_rows * decay_factors[:, :, None],
        value_matrix_rows,
        precision=exact_result,
    )
    return (memory_state, output_rows)


def chain(earlier, later):
    return (earlier[0] * later[0], earlier[1] * later[0][:, None, None] + later[1])


def shards(
    tokens,
    norm_gain,
    ret_query,
    ret_key,
    ret_value,
    att_query,
    att_key,
    att_value,
    log_decay,
    start_state,
    ret_gain,
    sink_logits,
    ret_out,
    att_out,
):
    gathered = lax.all_gather(tokens[0], "tp", axis=1, tiled=True)
    row_count = gathered.shape[0]
    as_float = gathered.astype(jnp.float32)
    normed = (
        as_float
        * lax.rsqrt(jnp.mean(as_float * as_float, axis=-1, keepdims=True) + epsilon)
        * norm_gain
    ).astype(jnp.bfloat16)
    offset = lax.axis_index("sp") * row_count
    positions = offset + jnp.arange(row_count, dtype=jnp.int32)
    weights = (ret_query, ret_key, ret_value, att_query, att_key, att_value)
    pieces = (
        lax.all_gather(weights[0], "sp", axis=0, tiled=True),
        lax.all_gather(weights[1], "sp", axis=0, tiled=True),
        lax.all_gather(weights[2], "sp", axis=0, tiled=True),
        lax.all_gather(weights[3], "sp", axis=0, tiled=True),
        lax.all_gather(weights[4], "sp", axis=0, tiled=True),
        lax.all_gather(weights[5], "sp", axis=0, tiled=True),
    )
    projected = tuple(
        (jnp.dot(normed, piece, preferred_element_type=jnp.float32) for piece in pieces)
    )
    rounded = tuple((product_f.astype(jnp.bfloat16) for product_f in projected))
    projected = rounded[:3]
    head_count = projected[0].shape[1] // DK
    queries = rotate(projected[0].astype(jnp.float32).reshape(row_count, head_count, DK), positions)
    keys_rot = rotate(
        projected[1].astype(jnp.float32).reshape(row_count, head_count, DK), positions
    ) * DK ** (-0.5)
    values_f = projected[2].astype(jnp.float32).reshape(row_count, head_count, DV)
    log_rates = log_decay[0]
    count = row_count // BLOCK

    def blocked(array):
        return array.reshape(count, BLOCK, head_count, array.shape[-1]).transpose(0, 2, 1, 3)

    rates_blocked = log_rates.reshape(head_count, count, BLOCK).transpose(1, 0, 2)
    local_state, pieces = lax.scan(
        block_step,
        jnp.zeros((head_count, DK, DV), jnp.float32),
        (blocked(queries), blocked(keys_rot), blocked(values_f), rates_blocked),
    )
    local_out = pieces.transpose(0, 2, 1, 3).reshape(row_count, head_count, DV)
    running_totals = jnp.cumsum(log_rates, axis=-1)
    device_decay = jnp.exp(running_totals[:, -1])
    identity = (jnp.ones((head_count,), jnp.float32), jnp.zeros((head_count, DK, DV), jnp.float32))
    prior_decay, prior_state = carried_in((device_decay, local_state), "sp", chain, identity)
    incoming = prior_state + prior_decay[:, None, None] * start_state[0]
    retained = local_out + jnp.einsum(
        "thd,hdv->thv",
        queries * jnp.exp(running_totals).T[:, :, None],
        incoming,
        precision=exact_result,
    )
    centred = retained - jnp.mean(retained, axis=-1, keepdims=True)
    variance = jnp.mean(centred * centred, axis=-1, keepdims=True)
    ret_hidden = (
        (centred * lax.rsqrt(variance + epsilon)).reshape(row_count, head_count * DV) * ret_gain
    ).astype(jnp.bfloat16)
    att_queries, att_keys, att_values = rounded[3:]
    kv_heads = att_keys.shape[1] // HD
    groups = att_queries.shape[1] // HD // kv_heads
    earlier_keys, earlier_values = passed_along(
        (att_keys[row_count - WINDOW :], att_values[row_count - WINDOW :]), "sp", 1
    )
    extended_keys = jnp.concatenate([earlier_keys, att_keys], axis=0)
    extended_values = jnp.concatenate([earlier_values, att_values], axis=0)
    windows = row_count // WINDOW

    def banded(array):
        earlier = array[:row_count].reshape(windows, WINDOW, kv_heads, HD)
        current = array[WINDOW:].reshape(windows, WINDOW, kv_heads, HD)
        return jnp.concatenate([earlier, current], axis=1)

    key_band = banded(extended_keys)
    value_band = banded(extended_values)
    grouped_q = att_queries.reshape(windows, WINDOW, kv_heads, groups, HD)
    score_matrix = jnp.einsum(
        "nqhgd,nkhd->nhgqk", grouped_q, key_band, preferred_element_type=jnp.float32
    ) * HD ** (-0.5)
    query_index = WINDOW + jnp.arange(WINDOW)
    key_index = jnp.arange(2 * WINDOW)
    allowed = (key_index[None, :] <= query_index[:, None]) & (
        query_index[:, None] - key_index[None, :] < WINDOW
    )
    key_place = offset - WINDOW + jnp.arange(windows)[:, None] * WINDOW + key_index[None, :]
    visible = (allowed[None] & (key_place >= 0)[:, None, :])[:, None, None]
    expo = jnp.exp(jnp.where(visible, score_matrix, -1e30))
    summed = jnp.sum(expo, axis=-1, keepdims=True) + jnp.exp(sink_logits).reshape(
        1, kv_heads, groups, 1, 1
    )
    probs = (expo / summed).astype(jnp.bfloat16)
    attended = jnp.einsum(
        "nhgqk,nkhd->nqhgd", probs, value_band, preferred_element_type=jnp.float32
    )
    att_hidden = attended.astype(jnp.bfloat16).reshape(row_count, kv_heads * groups * HD)
    ret_width = ret_hidden.shape[1]
    joined = jnp.concatenate([ret_hidden, att_hidden], axis=1)[None]
    piece = lax.all_gather(joined, "fs", axis=0, tiled=True)
    product = jnp.einsum(
        "srh,hd->srd", piece[:, :, :ret_width], ret_out, preferred_element_type=jnp.float32
    )
    product = product + jnp.einsum(
        "srh,hd->srd", piece[:, :, ret_width:], att_out, preferred_element_type=jnp.float32
    )
    partial_rows = product.astype(jnp.bfloat16)
    regrouped = lax.all_to_all(partial_rows, "fs", split_axis=0, concat_axis=2, tiled=True)
    mixed = lax.psum_scatter(
        regrouped[0].astype(jnp.float32).astype(jnp.bfloat16), "tp", scatter_dimension=1, tiled=True
    )
    return mixed[None]


def solution(mesh):
    placed = (
        P("fs", "sp", "tp"),
        P(),
        P("sp", "tp"),
        P("sp", "tp"),
        P("sp", "tp"),
        P("sp", "tp"),
        P("sp", "tp"),
        P("sp", "tp"),
        P("fs", "tp", "sp"),
        P("fs", "tp", None, None),
        P("tp"),
        P("tp"),
        P("tp", "fs"),
        P("tp", "fs"),
    )
    return jax.shard_map(
        shards, mesh=mesh, in_specs=placed, out_specs=P("fs", "sp", "tp"), check_vma=False
    )
```

profile of v0, /device:TPU:0, one launch (start us, length us, event | category | flops | bytes accessed | tf_op | source)
XLA Modules:
  0.0 330.0 jit_solution(6295431087866726067)
XLA Ops:
  13.0 13.6 %all-reduce = bf16[8]{0:T(256)(128)(2,1)S(1)} all-reduce(bf16[8]{0:T(256)(128)(2,1)S(1)} %dynamic-update-slice), channel_id=3, replica_groups=mesh['sp'=4,'fs'=4,'tp'=2] {'sp'}, use_global_device_ids=true, to_apply=%add | all-reduce | flops 8 | bytes 32
  26.6 18.4 %all_gather.42 = bf16[2048,128]{1,0:T(8,128)(2,1)S(1)} all-gather(bf16[512,128]{1,0:T(8,128)(2,1)S(1)} %copy-done.12), channel_id=1, replica_groups=mesh['sp'=4,'fs'=4,'tp'=2] {'sp'}, dimensions={0}, use_global_device_ids=true | all-gather | bytes 655360 | tf_op jit(solution)/shard_map/all_gather | solution.py:127
  45.7 21.2 %all_gather.41 = bf16[2048,128]{1,0:T(8,128)(2,1)} all-gather(bf16[512,128]{1,0:T(8,128)(2,1)S(1)} %copy-done.13), channel_id=1, replica_groups=mesh['sp'=4,'fs'=4,'tp'=2] {'sp'}, dimensions={0}, use_global_device_ids=true | all-gather | bytes 655360 | tf_op jit(solution)/shard_map/all_gather | solution.py:128
  66.9 1.2 multiply_cosine_fusion
  68.9 1.6 fusion.25
  70.5 1.7 convolution_convert_fusion.5
  72.9 2.6 collective-permute-start.1
  75.5 5.5 %all-gather.12.cloned.1.call-done = bf16[2048,512]{1,0:T(8,128)(2,1)} async-done(((bf16[512,512]{1,0:T(8,128)(2,1)}), bf16[2048,512]{1,0:T(8,128)(2,1)}) %all-gather.12.cloned.1.call-update) | async-done | bytes 2097168 | tf_op jit(solution)/shard_map/all_gather | solution.py:124
  80.9 2.3 fusion.31
  83.6 44.0 %all-gather.16.cloned.1.call-done = bf16[2048,512]{1,0:T(8,128)(2,1)} async-done(((bf16[512,512]{1,0:T(8,128)(2,1)}), bf16[2048,512]{1,0:T(8,128)(2,1)}) %all-gather.16.cloned.1.call-update) | async-done | bytes 2097168 | tf_op jit(solution)/shard_map/all_gather | solution.py:123
  127.6 2.7 fusion.33
  131.4 42.1 %all-gather.14.cloned.1.call-done = bf16[2048,512]{1,0:T(8,128)(2,1)} async-done(((bf16[512,512]{1,0:T(8,128)(2,1)}), bf16[2048,512]{1,0:T(8,128)(2,1)}) %all-gather.14.cloned.1.call-update) | async-done | bytes 2097168 | tf_op jit(solution)/shard_map/all_gather | solution.py:125
  173.6 2.7 fusion.32
  176.6 1.3 fusion.65
  178.9 6.7 %while.29 = (s32[]{:T(128)}, f32[2,256,256]{2,1,0:T(8,128)S(1)}, f32[2,2,128,256]{3,2,1,0:T(8,128)}, f32[2,2,128]{2,1,0:T(2,128)S(1)}, f32[2,2,128,256]{3,2,0,1:...) while((s32[]{:T(128)}, f32[2,256,256]{2,1,0:T(8,128)S(1)}, ...), condition=%wide.region_3.4_spmd.clone, body=%wide.region_1.3_spmd.clone.sunk | while | flops 604880896 | bytes 4242084 | solution.py:148
  180.2 1.2 fusion.95
  183.6 1.2 fusion.95
  186.4 1.9 convolution_convert_fusion.6
  188.6 2.3 collective-permute-start
  193.2 1.3 copy.65
  194.9 24.5 %all-gather.18.cloned.1.call-done = bf16[2048,512]{1,0:T(8,128)(2,1)} async-done(((bf16[512,512]{1,0:T(8,128)(2,1)}), bf16[2048,512]{1,0:T(8,128)(2,1)}) %all-gather.18.cloned.1.call-update) | async-done | bytes 2097168 | tf_op jit(solution)/shard_map/all_gather | solution.py:126
  219.5 2.3 convolution_convert_fusion.1
  223.8 25.1 %all-gather.22.cloned.1.call-done = bf16[8,256,256]{2,1,0:T(8,128)(2,1)} async-done(((bf16[2,256,256]{2,1,0:T(8,128)(2,1)}), bf16[8,256,256]{2,1,0:T(8,128)(2,1)}) %all-gather.22.cloned.1.call-update) | async-done | bytes 1048592 | tf_op jit(solution)/shard_map/all_gather | solution.py:18
  248.9 4.6 %while.30 = (s32[]{:T(128)}, f32[2]{0:T(128)S(1)}, f32[2,256,256]{2,1,0:T(8,128)S(1)}, s32[]{:T(128)}, bf16[4,2]{1,0:T(4,128)(2,1)S(1)}, /*index=5*/bf16[4,2,256,256]{3,2,1,0:T(8,128)(2,1)}, s32[]{:T(128)}, s32[]{:T(128)}) while((s32[]{:T(128)}, f32[2]{0:T(128)S(1)}, f32[2,256,256]{2,1,0:T(8,128)S(1)}, s32[]{:T(128)}, ...), condition=%wide.region_7.8_spmd.clone, body=%wide.region_6.7_spmd.clone.sunk | while | flops 655372 | bytes 1310871 | solution.py:35
  248.9 1.2 fusion.96
  253.6 1.2 fusion.67
  255.9 34.5 %all-gather.24.cloned.1.call-done = bf16[1024,1024]{0,1:T(8,128)(2,1)} async-done(((bf16[256,1024]{0,1:T(8,128)(2,1)}), bf16[1024,1024]{0,1:T(8,128)(2,1)}) %all-gather.24.cloned.1.call-update) | async-done | bytes 2097168 | tf_op jit(solution)/shard_map/all_gather | solution.py:209
  290.4 2.9 copy.81
  295.1 16.7 %all_to_all.15 = bf16[4,256,512]{2,1,0:T(8,128)(2,1)S(1)} all-to-all(bf16[4,256,512]{2,1,0:T(8,128)(2,1)S(1)} %add_convert_fusion), channel_id=1, replica_groups=mesh['sp'=4,'fs'=4,'tp'=2] {'fs'}, dimensions={0} | all-to-all | bytes 2097152 | tf_op jit(solution)/shard_map/all_to_all | solution.py:217
  311.8 1.3 copy.82
  313.1 8.0 %reduce-scatter.2.cloned.1.call-done = bf16[256,1024]{0,1:T(8,128)(2,1)} async-done(((bf16[256,2048]{0,1:T(8,128)(2,1)}), bf16[256,1024]{0,1:T(8,128)(2,1)}) %reduce-scatter.2.cloned.1.call-update) | async-done | bytes 524304 | tf_op jit(solution)/shard_map/reduce_scatter | solution.py:218
  321.1 2.0 copy.83
  (154 shorter events, 26.8 us)
Async XLA Ops:
  6.5 286.8 %copy-start = (bf16[512,512]{1,0:T(8,128)(2,1)S(1)}, bf16[512,512]{1,0:T(8,128)(2,1)}, u32[]{:S(2)}) copy-start(bf16[512,512]{1,0:T(8,128)(2,1)} %param.30) | copy-start | bytes 1572868
  6.5 4.8 %copy-start.23 = (u32[32]{0:T(128)S(1)}, u32[32]{0:T(128)}, u32[]{:S(2)}) copy-start(u32[32]{0:T(128)} %constant.93) | copy-start | bytes 388
  6.5 3.5 %copy-start.15 = (f32[1,2,256]{2,1,0:T(2,128)S(1)}, f32[1,2,256]{2,1,0:T(2,128)}, u32[]{:S(2)}) copy-start(f32[1,2,256]{2,1,0:T(2,128)} %param.26) | copy-start | bytes 6148
  6.5 20.1 %copy-start.12 = (bf16[512,128]{1,0:T(8,128)(2,1)S(1)}, bf16[512,128]{1,0:T(8,128)(2,1)}, u32[]{:S(2)}) copy-start(bf16[512,128]{1,0:T(8,128)(2,1)} %param.24) | copy-start | bytes 393220
  6.5 38.6 %copy-start.22 = (f32[8]{0:T(128)S(1)}, f32[8]{0:T(128)}, u32[]{:S(2)}) copy-start(f32[8]{0:T(128)} %param.29) | copy-start | bytes 100
  6.5 39.2 %copy-start.13 = (bf16[512,128]{1,0:T(8,128)(2,1)S(1)}, bf16[512,128]{1,0:T(8,128)(2,1)}, u32[]{:S(2)}) copy-start(bf16[512,128]{1,0:T(8,128)(2,1)} %param.25) | copy-start | bytes 393220
  6.6 62.3 %all-gather.20.cloned.1.call-start = ((), (), s32[]{:S(2)}) async-start(), calls=%async_computation.7 | async-start | bytes 1572864 | tf_op jit(solution)/shard_map/all_gather | solution.py:111
  7.3 73.6 %all-gather.12.cloned.1.call-start = ((), (), s32[]{:S(2)}) async-start(), calls=%async_computation.2 | async-start | bytes 2621440 | tf_op jit(solution)/shard_map/all_gather | solution.py:124
  8.0 62.5 %copy-start.20 = (f32[2048]{0:T(1024)S(1)}, f32[2048]{0:T(1024)}, u32[]{:S(2)}) copy-start(f32[2048]{0:T(1024)} %param.19) | copy-start | bytes 24580
  8.1 119.6 %all-gather.16.cloned.1.call-start = ((), (), s32[]{:S(2)}) async-start(), calls=%async_computation.4 | async-start | bytes 2621440 | tf_op jit(solution)/shard_map/all_gather | solution.py:123
  8.8 164.8 %all-gather.14.cloned.1.call-start = ((), (), s32[]{:S(2)}) async-start(), calls=%async_computation.3 | async-start | bytes 2621440 | tf_op jit(solution)/shard_map/all_gather | solution.py:125
  9.4 210.1 %all-gather.18.cloned.1.call-start = ((), (), s32[]{:S(2)}) async-start(), calls=%async_computation.5 | async-start | bytes 2621440 | tf_op jit(solution)/shard_map/all_gather | solution.py:126
  10.0 238.9 %all-gather.22.cloned.1.call-start = ((), (), s32[]{:S(2)}) async-start(), calls=%async_computation.8 | async-start | bytes 1310720 | tf_op jit(solution)/shard_map/all_gather | solution.py:18
  68.9 12.1 %copy-start.5 = (bf16[1,256,2048]{2,1,0:T(8,128)(2,1)S(1)}, bf16[1,256,2048]{2,1,0:T(8,128)(2,1)}, u32[]{:S(2)}) copy-start(bf16[1,256,2048]{2,1,0:T(8,128)(2,1)} %all-gather.20.cloned.1.call-done) | copy-start | bytes 3145732
  70.5 103.1 %copy-start.18 = (f32[256]{0:T(256)}, f32[256]{0:T(256)S(1)}, u32[]{:S(2)}) copy-start(f32[256]{0:T(256)S(1)} %add_rsqrt_fusion.1) | copy-start | bytes 3076
  72.2 11.0 %copy-start.10 = (bf16[256,128]{1,0:T(8,128)(2,1)}, bf16[256,128]{1,0:T(8,128)(2,1)S(1)}, u32[]{:S(2)}) copy-start(bf16[256,128]{1,0:T(8,128)(2,1)S(1)} %convolution_convert_fusion.5) | copy-start | bytes 196612
  72.9 118.2 %collective-permute-start.1 = (bf16[128,128]{1,0:T(8,128)(2,1)}, bf16[128,128]{1,0:T(8,128)(2,1)}, u32[]{:S(2)}, u32[]{:S(2)}) collective-permute-start(bf16[128,128]{1,0:T(8,128)(2,1)} %slice.64), channel_id=1, source_target_pairs={{0,8},{8,16},{16,24},{1,9},{9,17},{17,25},{2,10},{10,18},{18,26},{... | collective-permute-start | bytes 98312 | tf_op jit(solution)/shard_map/ppermute | solution.py:41
  176.6 1.3 copy-start.8
  178.8 7.6 %copy-start.19 = (f32[256]{0:T(256)S(1)}, f32[256]{0:T(256)}, u32[]{:S(2)}) copy-start(f32[256]{0:T(256)} %copy-done.18) | copy-start | bytes 3076
  178.8 7.6 %copy-start.21 = (f32[2048]{0:T(1024)S(1)}, f32[2048]{0:T(1024)}, u32[]{:S(2)}) copy-start(f32[2048]{0:T(1024)} %param.19) | copy-start | bytes 24580
  185.6 2.7 copy-start.11
  186.4 104.1 %all-gather.24.cloned.1.call-start = ((), (), s32[]{:S(2)}) async-start(), calls=%async_computation.9 | async-start | bytes 2621440 | tf_op jit(solution)/shard_map/all_gather | solution.py:209
  188.3 31.2 %copy-start.6 = (bf16[1,256,2048]{2,1,0:T(8,128)(2,1)S(1)}, bf16[1,256,2048]{2,1,0:T(8,128)(2,1)}, u32[]{:S(2)}) copy-start(bf16[1,256,2048]{2,1,0:T(8,128)(2,1)} %all-gather.20.cloned.1.call-done) | copy-start | bytes 3145732
  188.6 4.3 %collective-permute-start = (bf16[128,128]{1,0:T(8,128)(2,1)S(1)}, bf16[128,128]{1,0:T(8,128)(2,1)S(1)}, u32[]{:S(2)}, u32[]{:S(2)}) collective-permute-start(bf16[128,128]{1,0:T(8,128)(2,1)S(1)} %slice.63), channel_id=1, source_target_pairs={{0,8},{8,16},{16,24},{1,9},{9,17},{17,25},{2,10},{10,18},{18,26},{... | collective-permute-start | bytes 98312 | tf_op jit(solution)/shard_map/ppermute | solution.py:41
  194.9 27.2 %copy-start.14 = (pred[2,128,256]{1,2,0:T(8,128)(4,1)S(1)}, pred[2,128,256]{1,2,0:T(8,128)(4,1)}, u32[]{:S(2)}) copy-start(pred[2,128,256]{1,2,0:T(8,128)(4,1)} %broadcast_and_fusion) | copy-start | bytes 196612
  221.8 1.0 copy-start.17
  248.9 4.6 %copy-start.2 = (f32[256,2,128]{2,0,1:T(8,128)S(1)}, f32[256,2,128]{2,0,1:T(8,128)}, u32[]{:S(2)}) copy-start(f32[256,2,128]{2,0,1:T(8,128)} %copy-done.1) | copy-start | bytes 786436
  248.9 4.6 %copy-start.4 = (f32[256,2,128]{2,0,1:T(8,128)S(1)}, f32[256,2,128]{2,0,1:T(8,128)}, u32[]{:S(2)}) copy-start(f32[256,2,128]{2,0,1:T(8,128)} %copy-done.3) | copy-start | bytes 786436
  248.9 4.6 %copy-start.9 = (f32[1,2,256,256]{3,2,1,0:T(8,128)S(1)}, f32[1,2,256,256]{3,2,1,0:T(8,128)}, u32[]{:S(2)}) copy-start(f32[1,2,256,256]{3,2,1,0:T(8,128)} %param.27) | copy-start | bytes 1572868
  253.5 1.3 copy-start.16
  255.9 65.2 %reduce-scatter.2.cloned.1.call-start = ((), (), s32[]{:S(2)}) async-start(), calls=%async_computation.6 | async-start | bytes 1572864 | tf_op jit(solution)/shard_map/reduce_scatter | solution.py:218
  293.3 1.0 copy-start.7
  (2 other events, 1.5 us)
Sparse Core Ops, SparseCore 0:
  8.9 11.7 all-gather.19
  22.3 58.6 all-gather.11
  82.5 45.0 all-gather.15
  129.1 44.4 all-gather.13
  175.0 44.4 all-gather.17
  220.9 27.9 all-gather.21
  256.0 34.4 all-gather.23
  313.2 7.8 reduce-scatter.1
where the time goes:
time: 331 us; the launch traced here: 330 us
  waiting for transfers between devices  188 us (57%)
  blocking collectives  69.8 us (21%)
  matrix products  23 us (7%)
  local copies, waits for them, and re-layouts  16.4 us (5%)
  between operations  14.8 us (4%)
  other arithmetic  12.8 us (4%)
  starting transfers between devices  5.19 us (2%)
    all_gather x1, waiting for transfers between devices, shards(): lax.all_gather(weights[0], 'sp', axis=0, tiled=True)  44 us
    all_gather x1, waiting for transfers between devices, shards(): lax.all_gather(weights[2], 'sp', axis=0, tiled=True)  42.1 us
    all_gather x1, waiting for transfers between devices, shards(): piece = lax.all_gather(joined, 'fs', axis=0, tiled=True)  34.5 us
    all_gather x1, waiting for transfers between devices, carried_in(): lax.all_gather(part.astype(kind), axis)  25.1 us
    all_gather x1, waiting for transfers between devices, shards(): lax.all_gather(weights[3], 'sp', axis=0, tiled=True)  24.5 us
    all_gather x1, blocking collectives, shards(): lax.all_gather(weights[5], 'sp', axis=0, tiled=True)  21.2 us
    all_gather x1, blocking collectives, shards(): lax.all_gather(weights[4], 'sp', axis=0, tiled=True)  18.4 us
    all_to_all x1, blocking collectives, shards(): lax.all_to_all(partial_rows, 'fs', split_axis=0, concat_axis=2, tiled=True)  16.7 us
  transfers between devices with their start and end apart: 10, of which 8 were waited for; matrix products, arithmetic and copies ran while one was open for 11% of the time, Pallas kernels for 0%

commit v1 on v0

--- a/solution.py
+++ b/solution.py
@@ -1,3 +1,4 @@
+import functools
 import jax
 import jax.numpy as jnp
 from jax import lax
@@ -10,6 +11,34 @@
 BLOCK = 128
 epsilon = 1e-06
 exact_result = lax.Precision.HIGHEST
+
+
+def lead_sizes_now(content, row_dim, pos_dim):
+    piece_next, e_next = (lax.psum(1, axis_name="fs"), lax.axis_index("fs"))
+    local_next = list(content.shape)
+    reply = content.shape[row_dim] // piece_next
+    local_next[row_dim] = reply
+    item_now = local_next[pos_dim]
+    local_next[pos_dim] = item_now * piece_next
+    formed = jnp.zeros(local_next, content.dtype)
+    ii = 0
+    while ii < piece_next:
+        t_next = lax.dynamic_slice_in_dim(content, (e_next ^ ii) * reply, reply, axis=row_dim)
+        if ii:
+            nodes = []
+            ix = 0
+            while ix < piece_next:
+                nodes.append((ix, ix ^ ii))
+                ix += 1
+            t_next = lax.ppermute(t_next, axis_name="fs", perm=nodes)
+        formed = lax.dynamic_update_slice_in_dim(
+            formed, t_next, (e_next ^ ii) * item_now, axis=pos_dim
+        )
+        ii += 1
+    return formed
+
+
+digits_supply_all = functools.partial(lead_sizes_now, row_dim=0, pos_dim=2)
 
 
 def carried_in(array, axis, combine, identity):
@@ -214,7 +243,7 @@
         "srh,hd->srd", piece[:, :, ret_width:], att_out, preferred_element_type=jnp.float32
     )
     partial_rows = product.astype(jnp.bfloat16)
-    regrouped = lax.all_to_all(partial_rows, "fs", split_axis=0, concat_axis=2, tiled=True)
+    regrouped = digits_supply_all(partial_rows)
     mixed = lax.psum_scatter(
         regrouped[0].astype(jnp.float32).astype(jnp.bfloat16), "tp", scatter_dimension=1, tiled=True
     )

time: 331 us -> 328 us (level)
  blocking collectives: 69.8 us -> 53 us
  waiting for transfers between devices: 188 us -> 196 us
  starting transfers between devices: 5.19 us -> 8.76 us
    all_to_all x1 -> x0, blocking collectives: 16.7 us -> none  [shards(): lax.all_to_all(partial_rows, 'fs', split_axis=0, concat_axis=2, tiled=True)]
    ppermute x0 -> x3, waiting for transfers between devices: none -> 10.1 us  [lead_sizes_now(): t_next = lax.ppermute(t_next, axis_name='fs', perm=nodes)]
    ppermute x0 -> x3, starting transfers between devices: none -> 3.55 us  [lead_sizes_now(): t_next = lax.ppermute(t_next, axis_name='fs', perm=nodes)]
  transfers between devices with their start and end apart: 10 -> 13, of which waited for: 8 -> 10; matrix products, arithmetic and copies ran while one was open for 11% -> 12% of each run, Pallas kernels for 0% -> 0%
where the time goes in v1:
time: 328 us; the launch traced here: 327 us
  waiting for transfers between devices  196 us (60%)
  blocking collectives  53 us (16%)
  matrix products  23.8 us (7%)
  local copies, waits for them, and re-layouts  18.1 us (6%)
  between operations  14.8 us (5%)
  other arithmetic  12.2 us (4%)
  starting transfers between devices  8.76 us (3%)
    all_gather x1, waiting for transfers between devices, shards(): lax.all_gather(weights[0], 'sp', axis=0, tiled=True)  44 us
    all_gather x1, waiting for transfers between devices, shards(): lax.all_gather(weights[2], 'sp', axis=0, tiled=True)  42.1 us
    all_gather x1, waiting for transfers between devices, shards(): piece = lax.all_gather(joined, 'fs', axis=0, tiled=True)  34.5 us
    all_gather x1, waiting for transfers between devices, carried_in(): lax.all_gather(part.astype(kind), axis)  24.2 us
    all_gather x1, waiting for transfers between devices, shards(): lax.all_gather(weights[3], 'sp', axis=0, tiled=True)  23.4 us
    all_gather x1, blocking collectives, shards(): lax.all_gather(weights[5], 'sp', axis=0, tiled=True)  21.1 us
    all_gather x1, blocking collectives, shards(): lax.all_gather(weights[4], 'sp', axis=0, tiled=True)  18.3 us
    dot_general x6, matrix products, shards(): jnp.dot(normed, piece, preferred_element_type=jnp.float32)  13.6 us
  transfers between devices with their start and end apart: 13, of which 10 were waited for; matrix products, arithmetic and copies ran while one was open for 12% of the time, Pallas kernels for 0%

profile of v1, /device:TPU:0, one launch (start us, length us, event | category | flops | bytes accessed | tf_op | source)
XLA Modules:
  0.0 327.3 jit_solution(3347074958839519074)
XLA Ops:
  12.8 13.6 %all-reduce = bf16[8]{0:T(256)(128)(2,1)S(1)} all-reduce(bf16[8]{0:T(256)(128)(2,1)S(1)} %dynamic-update-slice), channel_id=3, replica_groups=mesh['sp'=4,'fs'=4,'tp'=2] {'sp'}, use_global_device_ids=true, to_apply=%add | all-reduce | flops 8 | bytes 32
  26.5 18.3 %all_gather.42 = bf16[2048,128]{1,0:T(8,128)(2,1)S(1)} all-gather(bf16[512,128]{1,0:T(8,128)(2,1)S(1)} %copy-done.11), channel_id=1, replica_groups=mesh['sp'=4,'fs'=4,'tp'=2] {'sp'}, dimensions={0}, use_global_device_ids=true | all-gather | bytes 655360 | tf_op jit(solution)/shard_map/all_gather | solution.py:156
  45.6 21.1 %all_gather.41 = bf16[2048,128]{1,0:T(8,128)(2,1)} all-gather(bf16[512,128]{1,0:T(8,128)(2,1)S(1)} %copy-done.12), channel_id=1, replica_groups=mesh['sp'=4,'fs'=4,'tp'=2] {'sp'}, dimensions={0}, use_global_device_ids=true | all-gather | bytes 655360 | tf_op jit(solution)/shard_map/all_gather | solution.py:157
  68.0 1.6 fusion.25
  69.6 1.7 convolution_convert_fusion.5
  72.0 2.7 collective-permute-start.1
  74.7 6.2 %all-gather.12.cloned.1.call-done = bf16[2048,512]{1,0:T(8,128)(2,1)} async-done(((bf16[512,512]{1,0:T(8,128)(2,1)}), bf16[2048,512]{1,0:T(8,128)(2,1)}) %all-gather.12.cloned.1.call-update) | async-done | bytes 2097168 | tf_op jit(solution)/shard_map/all_gather | solution.py:153
  80.8 2.3 fusion.31
  83.5 44.0 %all-gather.16.cloned.1.call-done = bf16[2048,512]{1,0:T(8,128)(2,1)} async-done(((bf16[512,512]{1,0:T(8,128)(2,1)}), bf16[2048,512]{1,0:T(8,128)(2,1)}) %all-gather.16.cloned.1.call-update) | async-done | bytes 2097168 | tf_op jit(solution)/shard_map/all_gather | solution.py:152
  127.5 2.7 fusion.33
  131.4 42.1 %all-gather.14.cloned.1.call-done = bf16[2048,512]{1,0:T(8,128)(2,1)} async-done(((bf16[512,512]{1,0:T(8,128)(2,1)}), bf16[2048,512]{1,0:T(8,128)(2,1)}) %all-gather.14.cloned.1.call-update) | async-done | bytes 2097168 | tf_op jit(solution)/shard_map/all_gather | solution.py:154
  173.5 2.7 fusion.32
  176.5 1.2 fusion.65
  178.7 6.8 %while.29 = (s32[]{:T(128)}, f32[2,256,256]{2,1,0:T(8,128)S(1)}, f32[2,2,128,256]{3,2,1,0:T(8,128)}, f32[2,2,128]{2,1,0:T(2,128)S(1)}, f32[2,2,128,256]{3,2,0,1:...) while((s32[]{:T(128)}, f32[2,256,256]{2,1,0:T(8,128)S(1)}, ...), condition=%wide.region_3.4_spmd.clone, body=%wide.region_1.3_spmd.clone.sunk | while | flops 604880896 | bytes 4242084 | solution.py:177
  180.1 1.2 fusion.95
  183.5 1.2 fusion.95
  186.3 1.9 convolution_convert_fusion.6
  189.1 2.2 collective-permute-start
  194.3 1.3 copy.63
  196.0 23.4 %all-gather.18.cloned.1.call-done = bf16[2048,512]{1,0:T(8,128)(2,1)} async-done(((bf16[512,512]{1,0:T(8,128)(2,1)}), bf16[2048,512]{1,0:T(8,128)(2,1)}) %all-gather.18.cloned.1.call-update) | async-done | bytes 2097168 | tf_op jit(solution)/shard_map/all_gather | solution.py:155
  219.4 2.4 convolution_convert_fusion.1
  222.0 1.5 fusion.29
  224.6 24.2 %all-gather.22.cloned.1.call-done = bf16[8,256,256]{2,1,0:T(8,128)(2,1)} async-done(((bf16[2,256,256]{2,1,0:T(8,128)(2,1)}), bf16[8,256,256]{2,1,0:T(8,128)(2,1)}) %all-gather.22.cloned.1.call-update) | async-done | bytes 1048592 | tf_op jit(solution)/shard_map/all_gather | solution.py:47
  248.8 4.6 %while.30 = (s32[]{:T(128)}, f32[2]{0:T(128)S(1)}, f32[2,256,256]{2,1,0:T(8,128)S(1)}, s32[]{:T(128)}, bf16[4,2]{1,0:T(4,128)(2,1)S(1)}, /*index=5*/bf16[4,2,256,256]{3,2,1,0:T(8,128)(2,1)}, s32[]{:T(128)}, s32[]{:T(128)}) while((s32[]{:T(128)}, f32[2]{0:T(128)S(1)}, f32[2,256,256]{2,1,0:T(8,128)S(1)}, s32[]{:T(128)}, ...), condition=%wide.region_7.8_spmd.clone, body=%wide.region_6.7_spmd.clone.sunk | while | flops 655372 | bytes 1310871 | solution.py:64
  248.8 1.2 fusion.96
  255.9 34.5 %all-gather.24.cloned.1.call-done = bf16[1024,1024]{0,1:T(8,128)(2,1)} async-done(((bf16[256,1024]{0,1:T(8,128)(2,1)}), bf16[1024,1024]{0,1:T(8,128)(2,1)}) %all-gather.24.cloned.1.call-update) | async-done | bytes 2097168 | tf_op jit(solution)/shard_map/all_gather | solution.py:238
  290.4 2.9 copy.79
  296.0 1.5 collective-permute-start.2
  298.1 1.5 collective-permute-start.4
  300.7 4.6 %collective-permute-done.2 = bf16[1,256,512]{2,1,0:T(8,128)(2,1)S(1)} collective-permute-done((bf16[1,256,512]{2,1,0:T(8,128)(2,1)S(1)}, bf16[1,256,512]{2,1,0:T(8,128)(2,1)S(1)}, u32[]{:S(2)}, u32[]{:S(2)}) %collective-permute-start.2) | collective-permute-done | bytes 262176 | tf_op jit(solution)/shard_map/ppermute | solution.py:33
  305.3 5.5 %collective-permute-done.3 = bf16[1,256,512]{2,1,0:T(8,128)(2,1)S(1)} collective-permute-done((bf16[1,256,512]{2,1,0:T(8,128)(2,1)S(1)}, bf16[1,256,512]{2,1,0:T(8,128)(2,1)S(1)}, u32[]{:S(2)}, u32[]{:S(2)}) %collective-permute-start.3) | collective-permute-done | bytes 262176 | tf_op jit(solution)/shard_map/ppermute | solution.py:33
  311.9 8.5 %reduce-scatter.2.cloned.1.call-done = bf16[256,1024]{1,0:T(8,128)(2,1)} async-done(((bf16[256,2048]{1,0:T(8,128)(2,1)}), bf16[256,1024]{1,0:T(8,128)(2,1)}) %reduce-scatter.2.cloned.1.call-update) | async-done | bytes 524304 | tf_op jit(solution)/shard_map/reduce_scatter | solution.py:247
  (163 shorter events, 32.8 us)
Async XLA Ops:
  6.5 286.7 %copy-start = (bf16[512,512]{1,0:T(8,128)(2,1)S(1)}, bf16[512,512]{1,0:T(8,128)(2,1)}, u32[]{:S(2)}) copy-start(bf16[512,512]{1,0:T(8,128)(2,1)} %param.30) | copy-start | bytes 1572868
  6.5 4.8 %copy-start.23 = (u32[32]{0:T(128)S(1)}, u32[32]{0:T(128)}, u32[]{:S(2)}) copy-start(u32[32]{0:T(128)} %constant.115) | copy-start | bytes 388
  6.5 3.5 %copy-start.16 = (f32[1,2,256]{2,1,0:T(2,128)S(1)}, f32[1,2,256]{2,1,0:T(2,128)}, u32[]{:S(2)}) copy-start(f32[1,2,256]{2,1,0:T(2,128)} %param.26) | copy-start | bytes 6148
  6.5 20.0 %copy-start.11 = (bf16[512,128]{1,0:T(8,128)(2,1)S(1)}, bf16[512,128]{1,0:T(8,128)(2,1)}, u32[]{:S(2)}) copy-start(bf16[512,128]{1,0:T(8,128)(2,1)} %param.24) | copy-start | bytes 393220
  6.5 38.4 %copy-start.22 = (f32[8]{0:T(128)S(1)}, f32[8]{0:T(128)}, u32[]{:S(2)}) copy-start(f32[8]{0:T(128)} %param.29) | copy-start | bytes 100
  6.5 39.0 %copy-start.12 = (bf16[512,128]{1,0:T(8,128)(2,1)S(1)}, bf16[512,128]{1,0:T(8,128)(2,1)}, u32[]{:S(2)}) copy-start(bf16[512,128]{1,0:T(8,128)(2,1)} %param.25) | copy-start | bytes 393220
  6.6 61.4 %all-gather.20.cloned.1.call-start = ((), (), s32[]{:S(2)}) async-start(), calls=%async_computation.6 | async-start | bytes 1572864 | tf_op jit(solution)/shard_map/all_gather | solution.py:140
  7.3 73.5 %all-gather.12.cloned.1.call-start = ((), (), s32[]{:S(2)}) async-start(), calls=%async_computation.1 | async-start | bytes 2621440 | tf_op jit(solution)/shard_map/all_gather | solution.py:153
  8.0 61.6 %copy-start.21 = (f32[2048]{0:T(1024)S(1)}, f32[2048]{0:T(1024)}, u32[]{:S(2)}) copy-start(f32[2048]{0:T(1024)} %param.19) | copy-start | bytes 24580
  8.1 119.5 %all-gather.16.cloned.1.call-start = ((), (), s32[]{:S(2)}) async-start(), calls=%async_computation.3 | async-start | bytes 2621440 | tf_op jit(solution)/shard_map/all_gather | solution.py:152
  8.8 164.7 %all-gather.14.cloned.1.call-start = ((), (), s32[]{:S(2)}) async-start(), calls=%async_computation.2 | async-start | bytes 2621440 | tf_op jit(solution)/shard_map/all_gather | solution.py:154
  9.4 210.0 %all-gather.18.cloned.1.call-start = ((), (), s32[]{:S(2)}) async-start(), calls=%async_computation.4 | async-start | bytes 2621440 | tf_op jit(solution)/shard_map/all_gather | solution.py:155
  10.0 238.8 %all-gather.22.cloned.1.call-start = ((), (), s32[]{:S(2)}) async-start(), calls=%async_computation.7 | async-start | bytes 1310720 | tf_op jit(solution)/shard_map/all_gather | solution.py:47
  68.0 12.8 %copy-start.7 = (bf16[1,256,2048]{2,1,0:T(8,128)(2,1)S(1)}, bf16[1,256,2048]{2,1,0:T(8,128)(2,1)}, u32[]{:S(2)}) copy-start(bf16[1,256,2048]{2,1,0:T(8,128)(2,1)} %all-gather.20.cloned.1.call-done) | copy-start | bytes 3145732
  69.6 116.7 %copy-start.19 = (f32[256]{0:T(256)}, f32[256]{0:T(256)S(1)}, u32[]{:S(2)}) copy-start(f32[256]{0:T(256)S(1)} %add_rsqrt_fusion.1) | copy-start | bytes 3076
  72.0 119.5 %collective-permute-start.1 = (bf16[128,128]{1,0:T(8,128)(2,1)}, bf16[128,128]{1,0:T(8,128)(2,1)}, u32[]{:S(2)}, u32[]{:S(2)}) collective-permute-start(bf16[128,128]{1,0:T(8,128)(2,1)} %slice.64), channel_id=1, source_target_pairs={{0,8},{8,16},{16,24},{1,9},{9,17},{17,25},{2,10},{10,18},{18,26},{... | collective-permute-start | bytes 98312 | tf_op jit(solution)/shard_map/ppermute | solution.py:70
  186.3 104.1 %all-gather.24.cloned.1.call-start = ((), (), s32[]{:S(2)}) async-start(), calls=%async_computation.8 | async-start | bytes 2621440 | tf_op jit(solution)/shard_map/all_gather | solution.py:238
  188.2 31.2 %copy-start.8 = (bf16[1,256,2048]{2,1,0:T(8,128)(2,1)S(1)}, bf16[1,256,2048]{2,1,0:T(8,128)(2,1)}, u32[]{:S(2)}) copy-start(bf16[1,256,2048]{2,1,0:T(8,128)(2,1)} %all-gather.20.cloned.1.call-done) | copy-start | bytes 3145732
  189.1 4.3 %collective-permute-start = (bf16[128,128]{1,0:T(8,128)(2,1)S(1)}, bf16[128,128]{1,0:T(8,128)(2,1)S(1)}, u32[]{:S(2)}, u32[]{:S(2)}) collective-permute-start(bf16[128,128]{1,0:T(8,128)(2,1)S(1)} %slice.63), channel_id=1, source_target_pairs={{0,8},{8,16},{16,24},{1,9},{9,17},{17,25},{2,10},{10,18},{18,26},{... | collective-permute-start | bytes 98312 | tf_op jit(solution)/shard_map/ppermute | solution.py:70
  192.3 27.1 %copy-start.20 = (f32[256]{0:T(256)S(1)}, f32[256]{0:T(256)}, u32[]{:S(2)}) copy-start(f32[256]{0:T(256)} %copy-done.19) | copy-start | bytes 3076
  196.0 26.1 %copy-start.13 = (bf16[2,128,2,64]{1,3,2,0:T(8,128)(2,1)S(1)}, bf16[2,128,2,64]{1,3,2,0:T(8,128)(2,1)}, u32[]{:S(2)}) copy-start(bf16[2,128,2,64]{1,3,2,0:T(8,128)(2,1)} %copy.74) | copy-start | bytes 196612
  221.7 1.8 copy-start.18
  221.7 1.9 copy-start.14
  221.7 1.9 copy-start.15
  248.8 4.6 %copy-start.4 = (f32[256,2,128]{2,0,1:T(8,128)S(1)}, f32[256,2,128]{2,0,1:T(8,128)}, u32[]{:S(2)}) copy-start(f32[256,2,128]{2,0,1:T(8,128)} %copy-done.3) | copy-start | bytes 786436
  248.8 4.6 %copy-start.6 = (f32[256,2,128]{2,0,1:T(8,128)S(1)}, f32[256,2,128]{2,0,1:T(8,128)}, u32[]{:S(2)}) copy-start(f32[256,2,128]{2,0,1:T(8,128)} %copy-done.5) | copy-start | bytes 786436
  248.8 4.6 %copy-start.10 = (f32[1,2,256,256]{3,2,1,0:T(8,128)S(1)}, f32[1,2,256,256]{3,2,1,0:T(8,128)}, u32[]{:S(2)}) copy-start(f32[1,2,256,256]{3,2,1,0:T(8,128)} %param.27) | copy-start | bytes 1572868
  253.4 1.3 copy-start.17
  255.8 64.6 %reduce-scatter.2.cloned.1.call-start = ((), (), s32[]{:S(2)}) async-start(), calls=%async_computation.5 | async-start | bytes 1572864 | tf_op jit(solution)/shard_map/reduce_scatter | solution.py:247
  296.0 9.2 %collective-permute-start.2 = (bf16[1,256,512]{2,1,0:T(8,128)(2,1)S(1)}, bf16[1,256,512]{2,1,0:T(8,128)(2,1)S(1)}, u32[]{:S(2)}, u32[]{:S(2)}) collective-permute-start(bf16[1,256,512]{2,1,0:T(8,128)(2,1)S(1)} %get-tuple-element.248), channel_id=1, source_target_pairs={{0,2},{2,0},{4,6},{6,4},{1,3},{3,1},{5,7},{7,5},{8,10},{10,8},{12,... | collective-permute-start | bytes 786440 | tf_op jit(solution)/shard_map/ppermute | solution.py:33
  297.6 13.2 %collective-permute-start.3 = (bf16[1,256,512]{2,1,0:T(8,128)(2,1)S(1)}, bf16[1,256,512]{2,1,0:T(8,128)(2,1)S(1)}, u32[]{:S(2)}, u32[]{:S(2)}) collective-permute-start(bf16[1,256,512]{2,1,0:T(8,128)(2,1)S(1)} %get-tuple-element.247), channel_id=1, source_target_pairs={{0,4},{2,6},{4,0},{6,2},{1,5},{3,7},{5,1},{7,3},{8,12},{10,14},{12... | collective-permute-start | bytes 786440 | tf_op jit(solution)/shard_map/ppermute | solution.py:33
  298.1 12.7 %collective-permute-start.4 = (bf16[1,256,512]{2,1,0:T(8,128)(2,1)S(1)}, bf16[1,256,512]{2,1,0:T(8,128)(2,1)S(1)}, u32[]{:S(2)}, u32[]{:S(2)}) collective-permute-start(bf16[1,256,512]{2,1,0:T(8,128)(2,1)S(1)} %get-tuple-element.246), channel_id=1, source_target_pairs={{0,6},{2,4},{4,2},{6,0},{1,7},{3,5},{5,3},{7,1},{8,14},{10,12},{12... | collective-permute-start | bytes 786440 | tf_op jit(solution)/shard_map/ppermute | solution.py:33
  (5 other events, 4.6 us)
Sparse Core Ops, SparseCore 0:
  8.9 11.7 all-gather.19
  22.3 58.5 all-gather.11
  82.4 45.0 all-gather.15
  129.0 44.4 all-gather.13
  174.9 44.4 all-gather.17
  220.8 27.9 all-gather.21
  255.9 34.4 all-gather.23
  312.0 8.3 reduce-scatter.1
